TPU v7x, 32 devices: a whole 2x2x4 slice. The times are simulated.
32 devices in a mesh: fs: 8 (over z, x), tp: 4 (over y, core).
Axes of the slice: x: 2, y: 2, z: 4, core: 2. Of those that a mesh axis runs over, the one named last changes fastest.
Arguments:
- saved_input: bfloat16 [2048, 4096], P('fs'), may hold values from -8 to 8
- query_cotangent: bfloat16 [2048, 2048], P('fs', 'tp'), may hold values from -6 to 6
- layer_cotangent: bfloat16 [2048, 4096], P('fs'), may hold values from -8 to 8
- mixed_heads: bfloat16 [2048, 2048], P('fs', 'tp'), may hold values from -6 to 6
- query_basis: bfloat16 [4096, 256], P('fs'), may hold values from -0.125 to 0.125
- output_basis: bfloat16 [4096, 256], P('fs'), may hold values from -0.125 to 0.125
- query_master: float32 [4096, 2048], P('fs', 'tp'), may hold values from -3 to 3
- output_master: float32 [4096, 2048], P('fs', 'tp'), may hold values from -3 to 3
- query_first: float32 [256, 2048], P('fs', 'tp'), may hold values from -6 to 6
- query_second: float32 [256, 2048], P('fs', 'tp'), may hold values from 0.25 to 4
- output_first: float32 [256, 2048], P('fs', 'tp'), may hold values from -6 to 6
- output_second: float32 [256, 2048], P('fs', 'tp'), may hold values from 0.25 to 4
Outputs:
- query_weight: float32 [4096, 2048], P('fs', 'tp')
- output_weight: float32 [4096, 2048], P('fs', 'tp')
- query_step: float32 [4096, 2048], P('fs', 'tp')
- output_step: float32 [4096, 2048], P('fs', 'tp')
- query_first_new: float32 [256, 2048], P('fs', 'tp')
- query_second_new: float32 [256, 2048], P('fs', 'tp')
- output_first_new: float32 [256, 2048], P('fs', 'tp')
- output_second_new: float32 [256, 2048], P('fs', 'tp')
- query_copy: bfloat16 [4096, 2048], P(None, 'tp')
- output_copy: bfloat16 [4096, 2048], P(None, 'tp')
All inputs are finite; a program needn't handle non-finite values.
Results may differ from a plain program's by a relative error of at most 0.0028.
Values may be sent and summed in bfloat16 or wider, within the bound.
A program may use at most 64 MiB of HBM per device.

v0:
```python
import jax
import jax.numpy as jnp
from jax import lax
from jax.sharding import PartitionSpec as P

QW = 2048
RANK = 256
beta_one = 0.8
beta_two = 0.9
rate = 0.1


def moment_update(low, factor, first, second):
    scaled = low * factor
    first_new = beta_one * first + (1.0 - beta_one) * scaled
    second_new = beta_two * second + (1.0 - beta_two) * scaled * scaled
    direction = (first_new / jnp.sqrt(second_new)).astype(jnp.bfloat16)
    return (first_new, second_new, direction)


def contract_tokens(left, right):
    return lax.dot_general(
        left,
        right,
        (((0,), (0,)), ((), ())),
        precision=lax.Precision.HIGHEST,
        preferred_element_type=jnp.float32,
    )


def per_device(
    saved_input,
    query_cotangent,
    layer_cotangent,
    mixed_heads,
    query_basis,
    output_basis,
    query_master,
    output_master,
    query_first,
    query_second,
    output_first,
    output_second,
):
    query_coords = jnp.dot(
        saved_input,
        lax.all_gather(query_basis, "fs", axis=0, tiled=True),
        preferred_element_type=jnp.float32,
    )
    output_coords = jnp.dot(
        layer_cotangent,
        lax.all_gather(output_basis, "fs", axis=0, tiled=True),
        preferred_element_type=jnp.float32,
    )
    query_part = contract_tokens(query_coords, query_cotangent.astype(jnp.float32))
    output_part = contract_tokens(output_coords, mixed_heads.astype(jnp.float32))
    query_low, output_low = (
        lax.psum_scatter(query_part, "fs", scatter_dimension=0, tiled=True),
        lax.psum_scatter(output_part, "fs", scatter_dimension=0, tiled=True),
    )
    local_squares = jnp.sum(query_low * query_low) + jnp.sum(output_low * output_low)
    total_squares = lax.psum(local_squares, ("fs", "tp"))
    factor = 1.0 / jnp.sqrt(1.0 + total_squares / (2.0 * RANK * QW))
    qf, qs, qdir = moment_update(query_low, factor, query_first, query_second)
    of, osec, odir = moment_update(output_low, factor, output_first, output_second)
    query_whole, output_whole = (
        lax.all_gather(qdir, "fs", axis=0, tiled=True),
        lax.all_gather(odir, "fs", axis=0, tiled=True),
    )
    query_step = jnp.dot(query_basis, query_whole, preferred_element_type=jnp.float32)
    output_step = jnp.dot(output_basis, output_whole, preferred_element_type=jnp.float32)
    query_weight = query_master - rate * query_step
    output_weight = output_master - rate * output_step
    query_copy, output_copy = (
        lax.all_gather(query_weight.astype(jnp.bfloat16), "fs", axis=0, tiled=True),
        lax.all_gather(output_weight.astype(jnp.bfloat16), "fs", axis=0, tiled=True),
    )
    return (
        query_weight,
        output_weight,
        query_step,
        output_step,
        qf,
        qs,
        of,
        osec,
        query_copy,
        output_copy,
    )


def solution(mesh):
    placed = (
        P("fs", None),
        P("fs", "tp"),
        P("fs", None),
        P("fs", "tp"),
        P("fs", None),
        P("fs", None),
        P("fs", "tp"),
        P("fs", "tp"),
        P("fs", "tp"),
        P("fs", "tp"),
        P("fs", "tp"),
        P("fs", "tp"),
    )
    return jax.shard_map(
        per_device,
        mesh=mesh,
        in_specs=placed,
        out_specs=(
            P("fs", "tp"),
            P("fs", "tp"),
            P("fs", "tp"),
            P("fs", "tp"),
            P("fs", "tp"),
            P("fs", "tp"),
            P("fs", "tp"),
            P("fs", "tp"),
            P(None, "tp"),
            P(None, "tp"),
        ),
        check_vma=False,
    )
```

profile of v0, /device:TPU:0, one launch (start us, length us, event | category | flops | bytes accessed | tf_op | source)
XLA Modules:
  0.0 486.5 jit_solution(8330795833223261178)
XLA Ops:
  7.2 0.0 copy-start
  7.2 0.0 all-gather.7.cloned.1.call-start
  7.2 0.7 all-gather.7.cloned.1.call-update
  7.9 0.0 all-gather.5.cloned.1.call-start
  8.0 0.7 all-gather.5.cloned.1.call-update
  8.7 0.0 copy-start.7
  8.7 0.0 reduce-scatter.5.cloned.1.call-start
  8.7 53.2 %all-gather.7.cloned.1.call-done = bf16[4096,256]{1,0:T(8,128)(2,1)} async-done(((bf16[512,256]{1,0:T(8,128)(2,1)}), bf16[4096,256]{1,0:T(8,128)(2,1)}) %all-gather.7.cloned.1.call-update) | async-done | bytes 2097168 | tf_op jit(solution)/shard_map/all_gather | solution.py:52
  62.0 0.0 copy-done
  62.0 2.3 fusion.8
  64.3 1.2 fusion.9
  65.5 0.0 reduce-scatter.5.cloned.1.call-update
  65.5 0.0 copy-start.4
  65.5 0.0 reduce-scatter.3.cloned.1.call-start
  65.6 46.2 %all-gather.5.cloned.1.call-done = bf16[4096,256]{1,0:T(8,128)(2,1)} async-done(((bf16[512,256]{1,0:T(8,128)(2,1)}), bf16[4096,256]{1,0:T(8,128)(2,1)}) %all-gather.5.cloned.1.call-update) | async-done | bytes 2097168 | tf_op jit(solution)/shard_map/all_gather | solution.py:47
  111.7 2.9 fusion.6
  114.7 0.0 copy-start.8
  114.7 0.0 copy-start.2
  114.7 2.2 fusion.7
  116.9 0.0 reduce-scatter.3.cloned.1.call-update
  116.9 0.0 all-gather.11.cloned.1.call-start
  117.0 59.9 %reduce-scatter.5.cloned.1.call-done = f32[32,512]{1,0:T(8,128)} async-done(((f32[256,512]{1,0:T(8,128)}), f32[32,512]{1,0:T(8,128)}) %reduce-scatter.5.cloned.1.call-update) | async-done | bytes 65552 | tf_op jit(solution)/shard_map/reduce_scatter | solution.py:59
  176.9 1.5 multiply_reduce_fusion
  178.4 63.9 %reduce-scatter.3.cloned.1.call-done = f32[32,512]{1,0:T(8,128)} async-done(((f32[256,512]{1,0:T(8,128)}), f32[32,512]{1,0:T(8,128)}) %reduce-scatter.3.cloned.1.call-update) | async-done | bytes 65552 | tf_op jit(solution)/shard_map/reduce_scatter | solution.py:58
  242.3 1.5 multiply_reduce_fusion.1
  245.1 0.0 copy-done.4
  245.1 1.3 copy.23
  246.4 39.9 %psum.7 = f32[]{:T(128)} all-reduce(f32[]{:T(128)S(6)} %add.24), channel_id=1, replica_groups=mesh['fs'=8,'tp'=4] {'fs','tp'}, use_global_device_ids=true, to_apply=%region_4.0 | all-reduce | flops 1 | bytes 8 | tf_op jit(solution)/shard_map/psum | solution.py:62
  287.0 1.5 multiply_convert_fusion
  288.5 30.7 %all_gather.21 = bf16[256,512]{1,0:T(8,128)(2,1)S(1)} all-gather(bf16[32,512]{1,0:T(8,128)(2,1)S(1)} %get-tuple-element.24), channel_id=1, replica_groups=mesh['fs'=8,'tp'=4] {'fs'}, dimensions={0}, use_global_device_ids=true | all-gather | bytes 294912 | tf_op jit(solution)/shard_map/all_gather | solution.py:68
  319.3 0.0 copy-done.2
  319.3 2.8 fusion.2
  322.1 0.0 all-gather.11.cloned.1.call-update
  322.1 0.0 all-gather.9.cloned.1.call-start
  322.1 2.6 copy.22
  324.7 0.0 copy-done.9
  324.7 1.5 multiply_convert_fusion.1
  326.3 32.0 %all_gather.20 = bf16[256,512]{1,0:T(8,128)(2,1)S(1)} all-gather(bf16[32,512]{1,0:T(8,128)(2,1)S(1)} %get-tuple-element.27), channel_id=1, replica_groups=mesh['fs'=8,'tp'=4] {'fs'}, dimensions={0}, use_global_device_ids=true | all-gather | bytes 294912 | tf_op jit(solution)/shard_map/all_gather | solution.py:67
  358.3 3.1 fusion.3
  361.4 0.0 all-gather.9.cloned.1.call-update
  361.4 2.6 copy.25
  364.0 1.3 copy.27
  365.3 2.6 copy.24
  367.9 1.3 copy.26
  369.2 28.7 %all-gather.11.cloned.1.call-done = bf16[4096,512]{0,1:T(8,128)(2,1)} async-done(((bf16[512,512]{0,1:T(8,128)(2,1)}), bf16[4096,512]{0,1:T(8,128)(2,1)}) %all-gather.11.cloned.1.call-update) | async-done | bytes 4194320 | tf_op jit(solution)/shard_map/all_gather | solution.py:76
  397.9 6.4 %copy.29 = bf16[4096,512]{1,0:T(8,128)(2,1)} copy(bf16[4096,512]{0,1:T(8,128)(2,1)} %all-gather.11.cloned.1.call-done) | data formatting | bytes 8388608
  404.3 68.9 %all-gather.9.cloned.1.call-done = bf16[4096,512]{0,1:T(8,128)(2,1)} async-done(((bf16[512,512]{0,1:T(8,128)(2,1)}), bf16[4096,512]{0,1:T(8,128)(2,1)}) %all-gather.9.cloned.1.call-update) | async-done | bytes 4194320 | tf_op jit(solution)/shard_map/all_gather | solution.py:75
  473.2 6.4 %copy.28 = bf16[4096,512]{1,0:T(8,128)(2,1)} copy(bf16[4096,512]{0,1:T(8,128)(2,1)} %all-gather.9.cloned.1.call-done) | data formatting | bytes 8388608
  (11 shorter events, 0.0 us)
Async XLA Ops:
  7.2 54.8 %copy-start = (bf16[256,4096]{1,0:T(8,128)(2,1)S(1)}, bf16[256,4096]{1,0:T(8,128)(2,1)}, u32[]{:S(2)}) copy-start(bf16[256,4096]{1,0:T(8,128)(2,1)} %param.14) | copy-start | bytes 6291460
  7.2 54.8 %all-gather.7.cloned.1.call-start = ((), (), s32[]{:S(2)}) async-start(), calls=%async_computation.4 | async-start | bytes 2359296 | tf_op jit(solution)/shard_map/all_gather | solution.py:52
  7.9 103.8 %all-gather.5.cloned.1.call-start = ((), (), s32[]{:S(2)}) async-start(), calls=%async_computation.2 | async-start | bytes 2359296 | tf_op jit(solution)/shard_map/all_gather | solution.py:47
  8.7 55.6 %copy-start.7 = (bf16[256,512]{1,0:T(8,128)(2,1)S(1)}, bf16[256,512]{1,0:T(8,128)(2,1)}, u32[]{:S(2)}) copy-start(bf16[256,512]{1,0:T(8,128)(2,1)} %param.15) | copy-start | bytes 786436
  8.7 168.2 %reduce-scatter.5.cloned.1.call-start = ((), (), s32[]{:S(2)}) async-start(), calls=%async_computation.5 | async-start | bytes 589824 | tf_op jit(solution)/shard_map/reduce_scatter | solution.py:59
  65.5 179.5 %copy-start.4 = (f32[512,512]{1,0:T(8,128)S(1)}, f32[512,512]{1,0:T(8,128)}, u32[]{:S(2)}) copy-start(f32[512,512]{1,0:T(8,128)} %param.19) | copy-start | bytes 3145732
  65.5 176.8 %reduce-scatter.3.cloned.1.call-start = ((), (), s32[]{:S(2)}) async-start(), calls=%async_computation.3 | async-start | bytes 589824 | tf_op jit(solution)/shard_map/reduce_scatter | solution.py:58
  114.7 172.3 %copy-start.8 = (f32[32,512]{1,0:T(8,128)S(1)}, f32[32,512]{1,0:T(8,128)}, u32[]{:S(2)}) copy-start(f32[32,512]{1,0:T(8,128)} %param.23) | copy-start | bytes 196612
  114.7 204.6 %copy-start.2 = (bf16[512,256]{1,0:T(8,128)(2,1)S(1)}, bf16[512,256]{1,0:T(8,128)(2,1)}, u32[]{:S(2)}) copy-start(bf16[512,256]{1,0:T(8,128)(2,1)} %param.17) | copy-start | bytes 786436
  116.9 281.0 %all-gather.11.cloned.1.call-start = ((), (), s32[]{:S(2)}) async-start(), calls=%async_computation.7 | async-start | bytes 4718592 | tf_op jit(solution)/shard_map/all_gather | solution.py:76
  176.8 110.2 %copy-start.6 = (f32[32,512]{1,0:T(8,128)S(1)}, f32[32,512]{1,0:T(8,128)}, u32[]{:S(2)}) copy-start(f32[32,512]{1,0:T(8,128)} %reduce-scatter.5.cloned.1.call-done) | copy-start | bytes 196612
  322.1 2.7 copy-start.5
  322.1 2.7 copy-start.9
  322.1 36.2 %copy-start.3 = (bf16[512,256]{1,0:T(8,128)(2,1)S(1)}, bf16[512,256]{1,0:T(8,128)(2,1)}, u32[]{:S(2)}) copy-start(bf16[512,256]{1,0:T(8,128)(2,1)} %param.16) | copy-start | bytes 786436
  322.1 151.1 %all-gather.9.cloned.1.call-start = ((), (), s32[]{:S(2)}) async-start(), calls=%async_computation.6 | async-start | bytes 4718592 | tf_op jit(solution)/shard_map/all_gather | solution.py:75
  365.3 2.6 copy-start.1
Sparse Core Ops, SparseCore 0:
  10.1 51.7 all-gather.6
  64.1 47.6 all-gather.4
  115.7 61.1 reduce-scatter.4
  180.6 61.6 reduce-scatter.2
  322.2 75.6 all-gather.10
  400.4 72.8 all-gather.8
where the time goes:
time: 487 us; the launch traced here: 486 us
  waiting for transfers between devices  322 us (66%)
  blocking collectives  103 us (21%)
  local copies, waits for them, and re-layouts  24.5 us (5%)
  between operations  16.2 us (3%)
  matrix products  14.6 us (3%)
  other arithmetic  6.02 us (1%)
    all_gather x1, waiting for transfers between devices, per_device(): lax.all_gather(query_weight.astype(jnp.bfloat16), 'fs', axis=0, tiled=True)  68.9 us
    reduce_scatter x1, waiting for transfers between devices, per_device(): lax.psum_scatter(query_part, 'fs', scatter_dimension=0, tiled=True)  63.9 us
    reduce_scatter x1, waiting for transfers between devices, per_device(): lax.psum_scatter(output_part, 'fs', scatter_dimension=0, tiled=True)  59.9 us
    all_gather x1, waiting for transfers between devices, per_device(): lax.all_gather(output_basis, 'fs', axis=0, tiled=True)  53.2 us
    all_gather x1, waiting for transfers between devices, per_device(): lax.all_gather(query_basis, 'fs', axis=0, tiled=True)  46.2 us
    psum x1, blocking collectives, per_device(): total_squares = lax.psum(local_squares, ('fs', 'tp'))  39.9 us
    all_gather x1, blocking collectives, per_device(): lax.all_gather(qdir, 'fs', axis=0, tiled=True)  32 us
    all_gather x1, blocking collectives, per_device(): lax.all_gather(odir, 'fs', axis=0, tiled=True)  30.7 us
  transfers between devices with their start and end apart: 6, of which 6 were waited for; matrix products, arithmetic and copies ran while one was open for 6% of the time, Pallas kernels for 0%

commit v1 on v0

--- a/solution.py
+++ b/solution.py
@@ -44,7 +44,9 @@
 ):
     query_coords = jnp.dot(
         saved_input,
-        lax.all_gather(query_basis, "fs", axis=0, tiled=True),
+        jnp.concatenate(
+            lax.all_to_all(jnp.stack([query_basis] * lax.axis_size("fs")), "fs", 0, 0), axis=0
+        ),
         preferred_element_type=jnp.float32,
     )
     output_coords = jnp.dot(

time: 487 us -> 467 us (0.959)
  waiting for transfers between devices: 322 us -> 293 us
  starting transfers between devices: 0.24 us -> 7.49 us
    all_gather x1 -> x0, waiting for transfers between devices: 46.2 us -> none  [per_device(): lax.all_gather(query_basis, 'fs', axis=0, tiled=True)]
    all_gather x1, waiting for transfers between devices: 68.9 us -> 28.5 us  [per_device(): lax.all_gather(query_weight.astype(jnp.bfloat16), 'fs', axis=0, tiled=True)]
    all_gather x1, waiting for transfers between devices: 28.7 us -> 68.3 us  [per_device(): lax.all_gather(output_weight.astype(jnp.bfloat16), 'fs', axis=0, tiled=True)]
    all_gather x1, waiting for transfers between devices: 53.2 us -> 75 us  [per_device(): lax.all_gather(output_basis, 'fs', axis=0, tiled=True)]
    all_to_all x0 -> x1, starting transfers between devices: none -> 7.28 us  [per_device(): lax.all_to_all(jnp.stack([query_basis] * lax.axis_size('fs')), 'fs', 0, 0)]
    unnamed x28 -> x30, local copies, waits for them, and re-layouts: 24.5 us -> 24.5 us
  transfers between devices with their start and end apart: 6 -> 6, of which waited for: 6 -> 5; matrix products, arithmetic and copies ran while one was open for 6% -> 7% of each run, Pallas kernels for 0% -> 0%
where the time goes in v1:
time: 467 us; the launch traced here: 466 us
  waiting for transfers between devices  293 us (63%)
  blocking collectives  103 us (22%)
  local copies, waits for them, and re-layouts  26.9 us (6%)
  between operations  15.9 us (3%)
  matrix products  13.7 us (3%)
  starting transfers between devices  7.49 us (2%)
  other arithmetic  6.02 us (1%)
    all_gather x1, waiting for transfers between devices, per_device(): lax.all_gather(output_basis, 'fs', axis=0, tiled=True)  75 us
    all_gather x1, waiting for transfers between devices, per_device(): lax.all_gather(output_weight.astype(jnp.bfloat16), 'fs', axis=0, tiled=True)  68.3 us
    reduce_scatter x1, waiting for transfers between devices, per_device(): lax.psum_scatter(query_part, 'fs', scatter_dimension=0, tiled=True)  64.2 us
    reduce_scatter x1, waiting for transfers between devices, per_device(): lax.psum_scatter(output_part, 'fs', scatter_dimension=0, tiled=True)  56.2 us
    psum x1, blocking collectives, per_device(): total_squares = lax.psum(local_squares, ('fs', 'tp'))  40 us
    all_gather x1, blocking collectives, per_device(): lax.all_gather(odir, 'fs', axis=0, tiled=True)  32.2 us
    all_gather x1, blocking collectives, per_device(): lax.all_gather(qdir, 'fs', axis=0, tiled=True)  30.7 us
    all_gather x1, waiting for transfers between devices, per_device(): lax.all_gather(query_weight.astype(jnp.bfloat16), 'fs', axis=0, tiled=True)  28.5 us
  transfers between devices with their start and end apart: 6, of which 5 were waited for; matrix products, arithmetic and copies ran while one was open for 7% of the time, Pallas kernels for 0%

profile of v1, /device:TPU:0, one launch (start us, length us, event | category | flops | bytes accessed | tf_op | source)
XLA Modules:
  0.0 466.0 jit_solution(12704365700582514130)
XLA Ops:
  7.2 0.0 copy-start
  7.2 0.0 all-gather.4.cloned.1.call-start
  7.2 0.7 all-gather.4.cloned.1.call-update
  7.9 2.4 stack.2
  10.3 7.3 %all-to-all-start = ((bf16[8,512,256]{2,1,0:T(8,128)(2,1)}), bf16[8,512,256]{2,1,0:T(8,128)(2,1)}, u32[]{:S(2)}, u32[]{:S(2)}) async-start(bf16[8,512,256]{2,1,0:T(8,128)(2,1)} %stack.2), calls=%async_computation | async-start | bytes 4194304 | tf_op jit(solution)/shard_map/all_to_all | solution.py:48
  17.6 0.0 reduce-scatter.5.cloned.1.call-start
  17.7 75.0 %all-gather.4.cloned.1.call-done = bf16[4096,256]{1,0:T(8,128)(2,1)} async-done(((bf16[512,256]{1,0:T(8,128)(2,1)}), bf16[4096,256]{1,0:T(8,128)(2,1)}) %all-gather.4.cloned.1.call-update) | async-done | bytes 2097168 | tf_op jit(solution)/shard_map/all_gather | solution.py:54
  92.7 0.0 copy-done
  92.7 2.3 fusion.8
  95.0 0.0 copy-done.7
  95.0 1.2 fusion.9
  96.2 0.0 reduce-scatter.5.cloned.1.call-update
  96.3 0.0 reduce-scatter.3.cloned.1.call-start
  96.3 0.0 all-to-all-done
  96.3 0.0 copy-start.8
  96.3 0.0 copy-start.4
  96.3 3.0 fusion.6
  99.4 0.0 copy-done.8
  99.4 0.0 copy-start.9
  99.4 0.0 copy-start.2
  99.4 1.2 fusion.7
  100.6 0.0 reduce-scatter.3.cloned.1.call-update
  100.6 0.0 all-gather.6.cloned.1.call-start
  100.7 56.2 %reduce-scatter.5.cloned.1.call-done = f32[32,512]{1,0:T(8,128)} async-done(((f32[256,512]{1,0:T(8,128)}), f32[32,512]{1,0:T(8,128)}) %reduce-scatter.5.cloned.1.call-update) | async-done | bytes 65552 | tf_op jit(solution)/shard_map/reduce_scatter | solution.py:61
  156.9 1.5 multiply_reduce_fusion
  158.4 64.2 %reduce-scatter.3.cloned.1.call-done = f32[32,512]{1,0:T(8,128)} async-done(((f32[256,512]{1,0:T(8,128)}), f32[32,512]{1,0:T(8,128)}) %reduce-scatter.3.cloned.1.call-update) | async-done | bytes 65552 | tf_op jit(solution)/shard_map/reduce_scatter | solution.py:60
  222.6 1.5 multiply_reduce_fusion.1
  225.4 1.3 copy.22
  226.7 40.0 %psum.7 = f32[]{:T(128)} all-reduce(f32[]{:T(128)S(6)} %add.24), channel_id=1, replica_groups=mesh['fs'=8,'tp'=4] {'fs','tp'}, use_global_device_ids=true, to_apply=%region_4.0 | all-reduce | flops 1 | bytes 8 | tf_op jit(solution)/shard_map/psum | solution.py:64
  267.4 1.5 multiply_convert_fusion.1
  268.9 30.7 %all_gather.16 = bf16[256,512]{1,0:T(8,128)(2,1)S(1)} all-gather(bf16[32,512]{1,0:T(8,128)(2,1)S(1)} %get-tuple-element.27), channel_id=1, replica_groups=mesh['fs'=8,'tp'=4] {'fs'}, dimensions={0}, use_global_device_ids=true | all-gather | bytes 294912 | tf_op jit(solution)/shard_map/all_gather | solution.py:69
  299.7 2.8 fusion.3
  302.5 0.0 all-gather.6.cloned.1.call-update
  302.5 0.0 all-gather.8.cloned.1.call-start
  302.6 2.6 copy.23
  305.1 0.0 copy-done.10
  305.1 1.5 multiply_convert_fusion
  306.7 32.2 %all_gather.17 = bf16[256,512]{1,0:T(8,128)(2,1)S(1)} all-gather(bf16[32,512]{1,0:T(8,128)(2,1)S(1)} %get-tuple-element.24), channel_id=1, replica_groups=mesh['fs'=8,'tp'=4] {'fs'}, dimensions={0}, use_global_device_ids=true | all-gather | bytes 294912 | tf_op jit(solution)/shard_map/all_gather | solution.py:70
  338.8 3.2 fusion.2
  342.0 0.0 all-gather.8.cloned.1.call-update
  342.0 2.6 copy.24
  344.6 1.3 copy.26
  345.9 2.6 copy.25
  348.5 1.3 copy.27
  349.8 28.5 %all-gather.6.cloned.1.call-done = bf16[4096,512]{0,1:T(8,128)(2,1)} async-done(((bf16[512,512]{0,1:T(8,128)(2,1)}), bf16[4096,512]{0,1:T(8,128)(2,1)}) %all-gather.6.cloned.1.call-update) | async-done | bytes 4194320 | tf_op jit(solution)/shard_map/all_gather | solution.py:77
  378.3 6.4 %copy.28 = bf16[4096,512]{1,0:T(8,128)(2,1)} copy(bf16[4096,512]{0,1:T(8,128)(2,1)} %all-gather.6.cloned.1.call-done) | data formatting | bytes 8388608
  384.7 68.3 %all-gather.8.cloned.1.call-done = bf16[4096,512]{0,1:T(8,128)(2,1)} async-done(((bf16[512,512]{0,1:T(8,128)(2,1)}), bf16[4096,512]{0,1:T(8,128)(2,1)}) %all-gather.8.cloned.1.call-update) | async-done | bytes 4194320 | tf_op jit(solution)/shard_map/all_gather | solution.py:78
  453.1 6.4 %copy.29 = bf16[4096,512]{1,0:T(8,128)(2,1)} copy(bf16[4096,512]{0,1:T(8,128)(2,1)} %all-gather.8.cloned.1.call-done) | data formatting | bytes 8388608
  (13 shorter events, 0.0 us)
Async XLA Ops:
  7.2 85.5 %copy-start = (bf16[256,4096]{1,0:T(8,128)(2,1)S(1)}, bf16[256,4096]{1,0:T(8,128)(2,1)}, u32[]{:S(2)}) copy-start(bf16[256,4096]{1,0:T(8,128)(2,1)} %param.14) | copy-start | bytes 6291460
  7.2 85.5 %all-gather.4.cloned.1.call-start = ((), (), s32[]{:S(2)}) async-start(), calls=%async_computation.4 | async-start | bytes 2359296 | tf_op jit(solution)/shard_map/all_gather | solution.py:54
  10.3 86.0 %all-to-all-start = ((bf16[8,512,256]{2,1,0:T(8,128)(2,1)}), bf16[8,512,256]{2,1,0:T(8,128)(2,1)}, u32[]{:S(2)}, u32[]{:S(2)}) async-start(bf16[8,512,256]{2,1,0:T(8,128)(2,1)} %stack.2), calls=%async_computation | async-start | bytes 4194304 | tf_op jit(solution)/shard_map/all_to_all | solution.py:48
  17.6 77.4 %copy-start.7 = (bf16[256,512]{1,0:T(8,128)(2,1)S(1)}, bf16[256,512]{1,0:T(8,128)(2,1)}, u32[]{:S(2)}) copy-start(bf16[256,512]{1,0:T(8,128)(2,1)} %param.15) | copy-start | bytes 786436
  17.6 139.3 %reduce-scatter.5.cloned.1.call-start = ((), (), s32[]{:S(2)}) async-start(), calls=%async_computation.5 | async-start | bytes 589824 | tf_op jit(solution)/shard_map/reduce_scatter | solution.py:61
  96.3 126.3 %reduce-scatter.3.cloned.1.call-start = ((), (), s32[]{:S(2)}) async-start(), calls=%async_computation.3 | async-start | bytes 589824 | tf_op jit(solution)/shard_map/reduce_scatter | solution.py:60
  96.3 3.1 copy-start.8
  96.3 129.1 %copy-start.4 = (f32[512,512]{1,0:T(8,128)S(1)}, f32[512,512]{1,0:T(8,128)}, u32[]{:S(2)}) copy-start(f32[512,512]{1,0:T(8,128)} %param.18) | copy-start | bytes 3145732
  99.4 168.0 %copy-start.9 = (f32[32,512]{1,0:T(8,128)S(1)}, f32[32,512]{1,0:T(8,128)}, u32[]{:S(2)}) copy-start(f32[32,512]{1,0:T(8,128)} %param.21) | copy-start | bytes 196612
  99.4 200.3 %copy-start.2 = (bf16[512,256]{1,0:T(8,128)(2,1)S(1)}, bf16[512,256]{1,0:T(8,128)(2,1)}, u32[]{:S(2)}) copy-start(bf16[512,256]{1,0:T(8,128)(2,1)} %param.16) | copy-start | bytes 786436
  100.6 277.7 %all-gather.6.cloned.1.call-start = ((), (), s32[]{:S(2)}) async-start(), calls=%async_computation.6 | async-start | bytes 4718592 | tf_op jit(solution)/shard_map/all_gather | solution.py:77
  222.6 44.8 %copy-start.6 = (f32[32,512]{1,0:T(8,128)S(1)}, f32[32,512]{1,0:T(8,128)}, u32[]{:S(2)}) copy-start(f32[32,512]{1,0:T(8,128)} %reduce-scatter.3.cloned.1.call-done) | copy-start | bytes 196612
  302.5 2.7 copy-start.5
  302.5 2.7 copy-start.10
  302.5 36.4 %copy-start.3 = (bf16[512,256]{1,0:T(8,128)(2,1)S(1)}, bf16[512,256]{1,0:T(8,128)(2,1)}, u32[]{:S(2)}) copy-start(bf16[512,256]{1,0:T(8,128)(2,1)} %param.17) | copy-start | bytes 786436
  302.5 150.6 %all-gather.8.cloned.1.call-start = ((), (), s32[]{:S(2)}) async-start(), calls=%async_computation.7 | async-start | bytes 4718592 | tf_op jit(solution)/shard_map/all_gather | solution.py:78
  345.9 2.6 copy-start.1
Sparse Core Ops, SparseCore 0:
  10.1 82.5 all-gather.3
  96.6 60.2 reduce-scatter.4
  160.8 61.6 reduce-scatter.2
  302.6 75.6 all-gather.5
  380.2 72.8 all-gather.7
